TPU v7x, 256 devices: a whole 4x4x8 slice. The times are simulated.
256 devices in a mesh: sp: 16 (over y, x), tp: 16 (over z, core).
Axes of the slice: x: 4, y: 4, z: 8, core: 2. Of those that a mesh axis runs over, the one named last changes fastest.
Arguments:
- queries: bfloat16 [16384, 1536], P('sp', 'tp'), may hold values from -34 to 34
- latent: bfloat16 [16384, 512], P('sp'), may hold values from -6 to 6
- rot_key: bfloat16 [16384, 32], P('sp'), may hold values from -34 to 34
- latent_gain: float32 [512], replicated, may hold values from 0.1 to 1.9
- key_up: bfloat16 [512, 1024], P(None, 'tp'), may hold values from -0.25 to 0.25
- value_up: bfloat16 [512, 1024], P(None, 'tp'), may hold values from -0.70710678 to 0.70710678
- query_gain: float32 [96], replicated, may hold values from 0.5 to 6
- key_gain: float32 [96], replicated, may hold values from 0.5 to 6
- out_gain: float32 [1024], replicated, may hold values from 0.1 to 1.9
- out_weight: bfloat16 [1024, 2048], replicated, may hold values from -0.1875 to 0.1875
- residual: bfloat16 [16384, 2048], P(('sp', 'tp')), may hold values from -6 to 6
- ffn_gain: float32 [2048], replicated, may hold values from 0.1 to 1.9
- routes: int32 [16384, 2], P(('sp', 'tp')), may hold values from 0 to 15, all different within a row; in each aligned block of 64 rows (0 to 63, 64 to 127, ...) at most 9 rows name the same one
- route_weights: float32 [16384, 2], P(('sp', 'tp')), may hold values from 0.2 to 1
- expert_gate: bfloat16 [16, 2048, 2048], P('sp', None, 'tp'), may hold values from -0.125 to 0.125
- expert_up: bfloat16 [16, 2048, 2048], P('sp', None, 'tp'), may hold values from -0.125 to 0.125
- expert_down: bfloat16 [16, 2048, 2048], P('sp', 'tp'), may hold values from -0.125 to 0.125
Outputs:
- layer_out: bfloat16 [16384, 2048], P(('sp', 'tp'))
Inputs may be any that keep to these rules, and one draw needn't show every extreme that they name: `routes`: the 2 experts of a token differ. Among the 64 rows of one device each expert is named by at most 9 rows, a bound that some block reaches.
All inputs are finite; a program needn't handle non-finite values.
Results may differ from a plain program's by a relative error of at most 0.02.
The roundings to bfloat16 on the way count: a program that leaves them out, or rounds other values in their place, can miss the bound.
Values may be sent and summed in bfloat16 or wider, within the bound.
A program may use at most 128 MiB of HBM per device.

v0:
```python
import jax
import jax.numpy as jnp
from jax import lax
from jax.sharding import PartitionSpec as P

D = 2048
NOPE = 64
ROPE = 32
VH = 64
TOPK = 2
QK = 96
epsilon = 1e-06
rope_base = 10000.0


def rms_scale(values):
    return lax.rsqrt(jnp.mean(values * values, axis=-1, keepdims=True) + epsilon)


def rotate_half(values, angles):
    half_dims = values.shape[-1] // 2
    first_half = values[..., :half_dims]
    second_half = values[..., half_dims:]
    cosine = jnp.cos(angles)
    sine_val = jnp.sin(angles)
    return jnp.concatenate(
        [
            first_half * cosine - second_half * sine_val,
            second_half * cosine + first_half * sine_val,
        ],
        axis=-1,
    )


def head_prepare(raw_rows, gain_vec, angles):
    normed_rows = raw_rows * rms_scale(raw_rows) * gain_vec
    turned_rows = rotate_half(normed_rows[..., NOPE:], angles[:, None, :])
    return jnp.concatenate([normed_rows[..., :NOPE], turned_rows], axis=-1).astype(jnp.bfloat16)


def slot_targets(route_rows, expert_total, slot_cap):
    flat_routes = route_rows.reshape(-1)
    one_hot = (flat_routes[:, None] == jnp.arange(expert_total, dtype=jnp.int32)[None, :]).astype(
        jnp.int32
    )
    earlier = jnp.cumsum(one_hot, axis=0) - one_hot
    rank_in = jnp.sum(earlier * one_hot, axis=1)
    return (flat_routes * slot_cap + rank_in).reshape(route_rows.shape)


def select_matrix(targets, slot_total):
    hits = targets[:, :, None] == jnp.arange(slot_total, dtype=jnp.int32)[None, None, :]
    return jnp.sum(hits.astype(jnp.bfloat16), axis=1)


def shards(
    queries,
    latent,
    rot_key,
    latent_gain,
    key_up,
    value_up,
    query_gain,
    key_gain,
    out_gain,
    out_weight,
    residual,
    ffn_gain,
    routes,
    route_weights,
    expert_gate,
    expert_up,
    expert_down,
):
    shard_len = queries.shape[0]
    local_heads = key_up.shape[1] // NOPE
    sp_count = lax.axis_size("sp")
    tp_count = lax.axis_size("tp")
    my_first = lax.axis_index("sp") * shard_len
    my_last = my_first + shard_len - 1
    positions = my_first + jnp.arange(shard_len, dtype=jnp.int32)
    inverse = rope_base ** (-jnp.arange(0, ROPE, 2, dtype=jnp.float32) / ROPE)
    angles = positions.astype(jnp.float32)[:, None] * inverse[None, :]
    lat_f32 = latent.astype(jnp.float32)
    normed_latent = (lat_f32 * rms_scale(lat_f32) * latent_gain).astype(jnp.bfloat16)
    key_nope = jnp.dot(normed_latent, key_up, preferred_element_type=jnp.float32).astype(
        jnp.bfloat16
    )
    value_rows = jnp.dot(normed_latent, value_up, preferred_element_type=jnp.float32).astype(
        jnp.bfloat16
    )
    shared = rot_key.astype(jnp.float32)[:, None, :]
    raw_keys = jnp.concatenate(
        [key_nope.astype(jnp.float32).reshape(shard_len, local_heads, NOPE), shared], axis=-1
    )
    key_rows = head_prepare(raw_keys, key_gain, angles)
    query_rows = head_prepare(
        queries.astype(jnp.float32).reshape(shard_len, local_heads, QK), query_gain, angles
    )
    query_heads = jnp.transpose(query_rows, (1, 0, 2))
    bundle = jnp.concatenate(
        [
            jnp.transpose(key_rows, (1, 2, 0)),
            jnp.transpose(value_rows.reshape(shard_len, local_heads, VH), (1, 2, 0)),
        ],
        axis=1,
    )
    score_scale = QK ** (-0.5)
    init_state = (
        jnp.full((local_heads, shard_len), -1e30, jnp.float32),
        jnp.zeros((local_heads, shard_len), jnp.float32),
        jnp.zeros((local_heads, shard_len, VH), jnp.float32),
    )
    key_piece = lax.all_gather(bundle, "sp", axis=2, tiled=True)
    block_count = key_piece.shape[2] // shard_len

    def one_block(block_index, running_state):
        first_key = block_index * shard_len

        def compute(inner):
            row_peak, row_total, weighted = inner
            key_part = lax.dynamic_slice_in_dim(key_piece, block_index * shard_len, shard_len, 2)
            scores = (
                jnp.einsum(
                    "hqc,hck->hqk",
                    query_heads,
                    key_part[:, :QK, :],
                    preferred_element_type=jnp.float32,
                )
                * score_scale
            )
            key_pos = first_key + jnp.arange(shard_len, dtype=jnp.int32)
            allowed = key_pos[None, None, :] <= positions[None, :, None]
            scores = jnp.where(allowed, scores, -1e30)
            new_peak = jnp.maximum(row_peak, jnp.max(scores, axis=2))
            exponent = jnp.where(allowed, jnp.exp(scores - new_peak[..., None]), 0.0)
            factor = jnp.exp(row_peak - new_peak)
            new_total = row_total * factor + jnp.sum(exponent, axis=2)
            contrib = jnp.einsum(
                "hqk,hvk->hqv",
                exponent.astype(jnp.bfloat16),
                key_part[:, QK:, :],
                preferred_element_type=jnp.float32,
            )
            return (new_peak, new_total, weighted * factor[..., None] + contrib)

        return lax.cond(first_key <= my_last, compute, lambda inner: inner, running_state)

    row_peak, row_total, weighted = lax.fori_loop(0, block_count, one_block, init_state)
    attended = (weighted / row_total[..., None]).astype(jnp.bfloat16)
    tok_count = residual.shape[0]
    head_major = jnp.transpose(attended, (1, 0, 2)).reshape(shard_len, local_heads * VH)
    token_rows = lax.all_to_all(head_major, "tp", split_axis=0, concat_axis=1, tiled=True).astype(
        jnp.float32
    )
    normed_rows = (token_rows * rms_scale(token_rows) * out_gain).astype(jnp.bfloat16)
    partials = jnp.einsum(
        "tgc,gcd->tgd",
        normed_rows.reshape(tok_count, tp_count, -1),
        out_weight.reshape(tp_count, -1, D),
        preferred_element_type=jnp.float32,
    )
    rounded = lax.optimization_barrier(partials.astype(jnp.bfloat16))
    mixed = jnp.sum(rounded.astype(jnp.float32), axis=1)
    middle = residual.astype(jnp.float32) + mixed
    ffn_input = (middle * rms_scale(middle) * ffn_gain).astype(jnp.bfloat16)
    slot_cap = max(2, 9 * tok_count * TOPK // (8 * sp_count))
    slot_total = sp_count * slot_cap
    targets = slot_targets(routes, sp_count, slot_cap)
    chooser = select_matrix(targets, slot_total)
    outbound = (
        jnp.einsum("ts,td->sd", chooser, ffn_input, preferred_element_type=jnp.float32)
        .astype(jnp.bfloat16)
        .reshape(sp_count, slot_cap, D)
    )
    arrived = lax.all_to_all(outbound, "sp", split_axis=0, concat_axis=0, tiled=True)
    item_count = arrived.shape[1]
    flat_rows = arrived.reshape(sp_count * item_count, D)
    row_block = lax.all_gather(flat_rows, "tp", axis=0, tiled=True)
    gate_pre = jnp.dot(row_block, expert_gate[0], preferred_element_type=jnp.float32)
    up_pre = jnp.dot(row_block, expert_up[0], preferred_element_type=jnp.float32)
    hidden = (jax.nn.silu(gate_pre) * up_pre).astype(jnp.bfloat16)
    served = lax.psum_scatter(
        jnp.dot(hidden, expert_down[0], preferred_element_type=jnp.float32).astype(jnp.bfloat16),
        "tp",
        scatter_dimension=0,
        tiled=True,
    ).reshape(sp_count, item_count, D)
    returned_rows = lax.all_to_all(served, "sp", split_axis=0, concat_axis=0, tiled=True).reshape(
        slot_total, D
    )
    picked = (
        jnp.take(returned_rows, targets.reshape(-1), axis=0)
        .reshape(tok_count, TOPK, D)
        .astype(jnp.float32)
    )
    moe_sum = jnp.sum(picked * route_weights[:, :, None], axis=1)
    return (middle + moe_sum).astype(jnp.bfloat16)


def solution(mesh):
    return jax.shard_map(
        shards,
        mesh=mesh,
        in_specs=(
            P("sp", "tp"),
            P("sp", None),
            P("sp", None),
            P(),
            P(None, "tp"),
            P(None, "tp"),
            P(),
            P(),
            P(),
            P(),
            P(("sp", "tp"), None),
            P(),
            P(("sp", "tp"), None),
            P(("sp", "tp"), None),
            P("sp", None, "tp"),
            P("sp", None, "tp"),
            P("sp", "tp", None),
        ),
        out_specs=P(("sp", "tp"), None),
        check_vma=False,
    )
```

profile of v0, /device:TPU:97, one launch (start us, length us, event | category | flops | bytes accessed | tf_op | source)
XLA Modules:
  0.0 451.1 jit_solution(6509418621641927697)
XLA Ops:
  6.6 1.6 fusion.21
  8.3 1.8 fusion.29
  11.0 1.0 fusion.42
  12.0 1.0 fusion.41
  16.1 61.9 %all-gather.3.cloned.1.call-done = bf16[1,160,16384]{2,1,0:T(8,128)(2,1)} async-done(((bf16[1,160,1024]{2,1,0:T(8,128)(2,1)}), bf16[1,160,16384]{2,1,0:T(8,128)(2,1)}) %all-gather.3.cloned.1.call-update) | async-done | bytes 5242896 | tf_op jit(solution)/shard_map/all_gather | solution.py:114
  78.0 9.9 %while.18 = (s32[]{:T(128)}, f32[1,1024]{1,0:T(1,128)S(1)}, f32[1,1024]{1,0:T(1,128)S(1)}, f32[1,1024,64]{1,2,0:T(8,128)S(1)}, s32[]{:T(128)}, /*index=5*/bf16[1...) while((s32[]{:T(128)}, f32[1,1024]{1,0:T(1,128)S(1)}, ...), condition=%wide.region_8.9_spmd.clone, body=%wide.region_3.8_spmd.clone.sunk | while | flops 352456704 | bytes 30515560 | solution.py:149
  78.0 9.1 %conditional.3 = ((f32[1,1024]{1,0:T(1,128)S(1)}, f32[1,1024]{1,0:T(1,128)S(1)}, f32[1,1024,64]{1,2,0:T(8,128)S(1)})) conditional(s32[]{:T(128)} %convert_element_type.207, (f32[1,1024]{1,0:T(1,128)S(1)}, f32[1,1024]{1,0:T(1,128)S(1)}, f32[1,1024,64]{1,2,0:T(8,128)S(1)}) %tuple.54, (s32[]{:T(128)}, s32[]{:T(128)}, s32[]{:T(128)}, ...), branch_computations={%region_4.0_spmd, %region_5.7_spmd} | conditional | flops 352456704 | bytes 30511242 | solution.py:147
  78.0 2.0 fusion.2
  80.1 2.0 copy-done.1
  82.1 1.5 fusion.4
  83.7 3.5 fusion.10
  89.0 7.8 %all-to-all-start = ((bf16[16,2,2048]{2,1,0:T(2,128)(2,1)}), bf16[16,2,2048]{2,1,0:T(2,128)(2,1)S(1)}, u32[]{:S(2)}, u32[]{:S(2)}) async-start(bf16[16,2,2048]{2,1,0:T(2,128)(2,1)} %reshape.512), calls=%async_computation | async-start | bytes 262144 | tf_op jit(solution)/shard_map/all_to_all | solution.py:153
  96.9 6.2 %all-to-all-done = bf16[16,2,2048]{2,1,0:T(2,128)(2,1)S(1)} async-done(((bf16[16,2,2048]{2,1,0:T(2,128)(2,1)}), bf16[16,2,2048]{2,1,0:T(2,128)(2,1)S(1)}, u32[]{:S(2)}, u32[]{:S(2)}) %all-to-all-start) | async-done | bytes 131104 | tf_op jit(solution)/shard_map/all_to_all | solution.py:153
  103.5 3.5 convert_bitcast_fusion
  108.8 156.9 %all_to_all.23 = bf16[16,9,2048]{2,1,0:T(8,128)(2,1)S(1)} all-to-all(bf16[16,9,2048]{2,1,0:T(8,128)(2,1)S(1)} %reshape.500), channel_id=1, replica_groups=mesh['sp'=16,'tp'=16] {'sp'}, dimensions={0} | all-to-all | bytes 1179648 | tf_op jit(solution)/shard_map/all_to_all | solution.py:176
  265.7 1.1 reshape.501
  267.1 57.2 %all-gather.5.cloned.1.call-done = bf16[2304,2048]{1,0:T(8,128)(2,1)} async-done(((bf16[144,2048]{1,0:T(8,128)(2,1)}), bf16[2304,2048]{1,0:T(8,128)(2,1)}) %all-gather.5.cloned.1.call-update) | async-done | bytes 9437200 | tf_op jit(solution)/shard_map/all_gather | solution.py:179
  324.3 5.3 %fusion.38 = f32[2304,128]{1,0:T(8,128)S(1)} fusion(bf16[2304,2048]{1,0:T(8,128)(2,1)} %all-gather.5.cloned.1.call-done, bf16[1,2048,128]{2,1,0:T(8,128)(2,1)} %param.35), kind=kOutput, calls=%fused_computation.53 | convolution fusion | flops 1207959552 | bytes 11141120 | tf_op jit(solution)/shard_map/dot_general | solution.py:180
  329.6 14.2 %convolution_convert_fusion = bf16[2304,2048]{1,0:T(8,128)(2,1)} fusion(bf16[2304,2048]{1,0:T(8,128)(2,1)} %all-gather.5.cloned.1.call-done, f32[2304,128]{1,0:T(8,128)S(1)} %fusion.38, bf16[1,128,2048]{2,1,0:T(8,128)(2,1)S(1)} %copy-done, bf16[1,2048,128]{2,1,0:T(8,128)(2,1)S(1)} %copy-done.5), kind=kOutput, calls=%fused_computation.23 | convolution fusion | flops 2422407168 | bytes 21102592 | tf_op jit(solution)/shard_map/dot_general | solution.py:184
  343.9 71.6 %reduce-scatter.2.cloned.1.call-done = bf16[144,2048]{1,0:T(8,128)(2,1)} async-done(((bf16[2304,2048]{1,0:T(8,128)(2,1)}), bf16[144,2048]{1,0:T(8,128)(2,1)}) %reduce-scatter.2.cloned.1.call-update) | async-done | bytes 589840 | tf_op jit(solution)/shard_map/reduce_scatter | solution.py:183
  415.5 2.3 reshape.502
  417.8 6.5 %all-to-all-start.2 = ((bf16[16,9,2048]{2,1,0:T(8,128)(2,1)}), bf16[16,9,2048]{2,1,0:T(8,128)(2,1)S(1)}, u32[]{:S(2)}, u32[]{:S(2)}) async-start(bf16[16,9,2048]{2,1,0:T(8,128)(2,1)} %reshape.502), calls=%async_computation.3 | async-start | bytes 2097152 | tf_op jit(solution)/shard_map/all_to_all | solution.py:189
  424.8 15.1 %all-to-all-done.2 = bf16[16,9,2048]{2,1,0:T(8,128)(2,1)S(1)} async-done(((bf16[16,9,2048]{2,1,0:T(8,128)(2,1)}), bf16[16,9,2048]{2,1,0:T(8,128)(2,1)S(1)}, u32[]{:S(2)}, u32[]{:S(2)}) %all-to-all-start.2) | async-done | bytes 589856 | tf_op jit(solution)/shard_map/all_to_all | solution.py:189
  441.4 2.3 multiply_reduce_fusion
  (116 shorter events, 10.6 us)
Async XLA Ops:
  6.5 323.1 %copy-start = (bf16[1,128,2048]{2,1,0:T(8,128)(2,1)S(1)}, bf16[1,128,2048]{2,1,0:T(8,128)(2,1)}, u32[]{:S(2)}) copy-start(bf16[1,128,2048]{2,1,0:T(8,128)(2,1)} %param.37) | copy-start | bytes 1572868
  6.5 6.4 %copy-start.3 = (bf16[1024,512]{1,0:T(8,128)(2,1)S(1)}, bf16[1024,512]{1,0:T(8,128)(2,1)}, u32[]{:S(2)}) copy-start(bf16[1024,512]{1,0:T(8,128)(2,1)} %param.22) | copy-start | bytes 3145732
  6.5 6.5 %copy-start.12 = (f32[512]{0:T(512)S(1)}, f32[512]{0:T(512)}, u32[]{:S(2)}) copy-start(f32[512]{0:T(512)} %param.24) | copy-start | bytes 6148
  6.5 7.0 %copy-start.4 = (bf16[1024,96]{0,1:T(8,128)(2,1)S(1)}, bf16[1024,96]{0,1:T(8,128)(2,1)}, u32[]{:S(2)}) copy-start(bf16[1024,96]{0,1:T(8,128)(2,1)} %param.21) | copy-start | bytes 589828
  6.5 6.5 %copy-start.11 = (bf16[512,64]{0,1:T(8,128)(2,1)S(1)}, bf16[512,64]{0,1:T(8,128)(2,1)}, u32[]{:S(2)}) copy-start(bf16[512,64]{0,1:T(8,128)(2,1)} %param.26) | copy-start | bytes 196612
  6.5 7.0 %copy-start.10 = (f32[96]{0:T(128)S(1)}, f32[96]{0:T(128)}, u32[]{:S(2)}) copy-start(f32[96]{0:T(128)} %param.27) | copy-start | bytes 1156
  6.6 71.4 %all-gather.3.cloned.1.call-start = ((), (), s32[]{:S(2)}) async-start(), calls=%async_computation.4 | async-start | bytes 5570560 | tf_op jit(solution)/shard_map/all_gather | solution.py:114
  8.3 6.8 %copy-start.8 = (f32[1024]{0:T(1024)S(1)}, f32[1024]{0:T(1024)}, u32[]{:S(2)}) copy-start(f32[1024]{0:T(1024)} %param.29) | copy-start | bytes 12292
  8.3 6.9 %copy-start.6 = (s32[64,2]{0,1:T(2,128)S(1)}, s32[64,2]{0,1:T(2,128)}, u32[]{:S(2)}) copy-start(s32[64,2]{0,1:T(2,128)} %param.33) | copy-start | bytes 1540
  80.1 2.0 copy-start.1
  89.0 14.1 %all-to-all-start = ((bf16[16,2,2048]{2,1,0:T(2,128)(2,1)}), bf16[16,2,2048]{2,1,0:T(2,128)(2,1)S(1)}, u32[]{:S(2)}, u32[]{:S(2)}) async-start(bf16[16,2,2048]{2,1,0:T(2,128)(2,1)} %reshape.512), calls=%async_computation | async-start | bytes 262144 | tf_op jit(solution)/shard_map/all_to_all | solution.py:153
  96.8 227.5 %all-gather.5.cloned.1.call-start = ((), (), s32[]{:S(2)}) async-start(), calls=%async_computation.5 | async-start | bytes 10027008 | tf_op jit(solution)/shard_map/all_gather | solution.py:179
  107.0 1.0 copy-start.2
  107.0 1.1 copy-start.7
  266.8 62.8 %copy-start.5 = (bf16[1,2048,128]{2,1,0:T(8,128)(2,1)S(1)}, bf16[1,2048,128]{2,1,0:T(8,128)(2,1)}, u32[]{:S(2)}) copy-start(bf16[1,2048,128]{2,1,0:T(8,128)(2,1)} %param.36) | copy-start | bytes 1572868
  266.8 148.7 %reduce-scatter.2.cloned.1.call-start = ((), (), s32[]{:S(2)}) async-start(), calls=%async_computation.6 | async-start | bytes 10027008 | tf_op jit(solution)/shard_map/reduce_scatter | solution.py:183
  343.8 80.8 %copy-start.9 = (f32[64,2]{0,1:T(2,128)S(1)}, f32[64,2]{0,1:T(2,128)}, u32[]{:S(2)}) copy-start(f32[64,2]{0,1:T(2,128)} %param.34) | copy-start | bytes 1540
  417.8 22.1 %all-to-all-start.2 = ((bf16[16,9,2048]{2,1,0:T(8,128)(2,1)}), bf16[16,9,2048]{2,1,0:T(8,128)(2,1)S(1)}, u32[]{:S(2)}, u32[]{:S(2)}) async-start(bf16[16,9,2048]{2,1,0:T(8,128)(2,1)} %reshape.502), calls=%async_computation.3 | async-start | bytes 2097152 | tf_op jit(solution)/shard_map/all_to_all | solution.py:189
Sparse Core Ops, SparseCore 0:
  14.9 62.9 all-gather.2
  266.9 57.2 all-gather.4
  344.0 71.4 reduce-scatter.1
where the time goes:
time: 452 us; the launch traced here: 451 us
  waiting for transfers between devices  212 us (47%)
  blocking collectives  157 us (35%)
  matrix products  31.3 us (7%)
  starting transfers between devices  14.6 us (3%)
  between operations  13.5 us (3%)
  other arithmetic  12 us (3%)
  local copies, waits for them, and re-layouts  9.85 us (2%)
    all_to_all x1, blocking collectives, shards(): lax.all_to_all(outbound, 'sp', split_axis=0, concat_axis=0, tiled=True)  157 us
    reduce_scatter x1, waiting for transfers between devices, shards(): lax.psum_scatter(jnp.dot(hidden, expert_down[0], preferred_element_type=j...  71.6 us
    all_gather x1, waiting for transfers between devices, shards(): key_piece = lax.all_gather(bundle, 'sp', axis=2, tiled=True)  61.9 us
    all_gather x1, waiting for transfers between devices, shards(): row_block = lax.all_gather(flat_rows, 'tp', axis=0, tiled=True)  57.2 us
    all_to_all x1, waiting for transfers between devices, shards(): lax.all_to_all(served, 'sp', split_axis=0, concat_axis=0, tiled=True)  15.1 us
    dot_general x1, matrix products, shards(): jnp.dot(hidden, expert_down[0], preferred_element_type=jnp.float32)  14.2 us
  transfers between devices with their start and end apart: 5, of which 5 were waited for; matrix products, arithmetic and copies ran while one was open for 0% of the time, Pallas kernels for 0%

commit v1 on v0

--- a/solution.py
+++ b/solution.py
@@ -176,7 +176,23 @@
     arrived = lax.all_to_all(outbound, "sp", split_axis=0, concat_axis=0, tiled=True)
     item_count = arrived.shape[1]
     flat_rows = arrived.reshape(sp_count * item_count, D)
-    row_block = lax.all_gather(flat_rows, "tp", axis=0, tiled=True)
+    n_shards = lax.axis_size("tp")
+    rows = []
+    for t in range(n_shards):
+        rows.append((t, (t + 1) % n_shards))
+    panels = []
+    for t in range(n_shards):
+        panels.append((t, (t - 1) % n_shards))
+    r1, before = ([flat_rows], [flat_rows])
+    for _ in range(n_shards // 2):
+        u_next = lax.ppermute(r1[-1], "tp", rows)
+        r1.append(u_next)
+    for _ in range((n_shards - 1) // 2):
+        before.append(lax.ppermute(before[-1], "tp", panels))
+    seen_now = jnp.concatenate([*r1[::-1], *before[1:]], axis=0)
+    row_block = jnp.roll(
+        seen_now, (lax.axis_index("tp") - n_shards // 2) * flat_rows.shape[0], axis=0
+    )
     gate_pre = jnp.dot(row_block, expert_gate[0], preferred_element_type=jnp.float32)
     up_pre = jnp.dot(row_block, expert_up[0], preferred_element_type=jnp.float32)
     hidden = (jax.nn.silu(gate_pre) * up_pre).astype(jnp.bfloat16)

time: 452 us -> 501 us (1.11)
  starting transfers between devices: 14.6 us -> 42.5 us
  local copies, waits for them, and re-layouts: 9.85 us -> 36.6 us
  waiting for transfers between devices: 212 us -> 205 us
    all_gather x1 -> x0, waiting for transfers between devices: 57.2 us -> none  [shards(): row_block = lax.all_gather(flat_rows, 'tp', axis=0, tiled=True)]
    ppermute x0 -> x15, waiting for transfers between devices: none -> 52.4 us  [the longest x8 47 us: shards(): u_next = lax.ppermute(r1[-1], 'tp', rows)]
    ppermute x0 -> x15, starting transfers between devices: none -> 28.1 us  [the longest x8 28.1 us: shards(): u_next = lax.ppermute(r1[-1], 'tp', rows)]
    unnamed x29 -> x80, local copies, waits for them, and re-layouts: 1.7 us -> 28.5 us
  transfers between devices with their start and end apart: 5 -> 19, of which waited for: 5 -> 16; matrix products, arithmetic and copies ran while one was open for 0% -> 3% of each run, Pallas kernels for 0% -> 0%
where the time goes in v1:
time: 501 us; the launch traced here: 499 us
  waiting for transfers between devices  205 us (41%)
  blocking collectives  157 us (31%)
  starting transfers between devices  42.5 us (8%)
  local copies, waits for them, and re-layouts  36.6 us (7%)
  matrix products  30.2 us (6%)
  between operations  14.1 us (3%)
  other arithmetic  12.9 us (3%)
    all_to_all x1, blocking collectives, shards(): lax.all_to_all(outbound, 'sp', split_axis=0, concat_axis=0, tiled=True)  157 us
    reduce_scatter x1, waiting for transfers between devices, shards(): lax.psum_scatter(jnp.dot(hidden, expert_down[0], preferred_element_type=j...  71.3 us
    all_gather x1, waiting for transfers between devices, shards(): key_piece = lax.all_gather(bundle, 'sp', axis=2, tiled=True)  60.5 us
    ppermute x8, waiting for transfers between devices, shards(): u_next = lax.ppermute(r1[-1], 'tp', rows)  47 us
    unnamed x80, local copies, waits for them, and re-layouts  28.5 us
    ppermute x8, starting transfers between devices, shards(): u_next = lax.ppermute(r1[-1], 'tp', rows)  28.1 us
    all_to_all x1, waiting for transfers between devices, shards(): lax.all_to_all(served, 'sp', split_axis=0, concat_axis=0, tiled=True)  15 us
    dot_general x1, matrix products, shards(): jnp.dot(hidden, expert_down[0], preferred_element_type=jnp.float32)  14.5 us
  transfers between devices with their start and end apart: 19, of which 16 were waited for; matrix products, arithmetic and copies ran while one was open for 3% of the time, Pallas kernels for 0%

profile of v1, /device:TPU:97, one launch (start us, length us, event | category | flops | bytes accessed | tf_op | source)
XLA Modules:
  0.0 499.4 jit_solution(3052412768450823033)
XLA Ops:
  19.4 60.5 %all-gather.2.cloned.1.call-done = bf16[1,160,16384]{2,1,0:T(8,128)(2,1)} async-done(((bf16[1,160,1024]{2,1,0:T(8,128)(2,1)}), bf16[1,160,16384]{2,1,0:T(8,128)(2,1)}) %all-gather.2.cloned.1.call-update) | async-done | bytes 5242896 | tf_op jit(solution)/shard_map/all_gather | solution.py:114
  80.0 9.9 %while.18 = (s32[]{:T(128)}, f32[1,1024]{1,0:T(1,128)S(1)}, f32[1,1024]{1,0:T(1,128)S(1)}, f32[1,1024,64]{1,2,0:T(8,128)S(1)}, s32[]{:T(128)}, /*index=5*/bf16[1...) while((s32[]{:T(128)}, f32[1,1024]{1,0:T(1,128)S(1)}, ...), condition=%wide.region_8.9_spmd.clone, body=%wide.region_3.8_spmd.clone.sunk | while | flops 352456704 | bytes 30515560 | solution.py:149
  80.0 9.1 %conditional.3 = ((f32[1,1024]{1,0:T(1,128)S(1)}, f32[1,1024]{1,0:T(1,128)S(1)}, f32[1,1024,64]{1,2,0:T(8,128)S(1)})) conditional(s32[]{:T(128)} %convert_element_type.206, (f32[1,1024]{1,0:T(1,128)S(1)}, f32[1,1024]{1,0:T(1,128)S(1)}, f32[1,1024,64]{1,2,0:T(8,128)S(1)}) %tuple.54, (s32[]{:T(128)}, s32[]{:T(128)}, s32[]{:T(128)}, ...), branch_computations={%region_4.0_spmd, %region_5.7_spmd} | conditional | flops 352456704 | bytes 30511242 | solution.py:147
  91.0 7.8 %all-to-all-start = ((bf16[16,2,2048]{2,1,0:T(2,128)(2,1)}), bf16[16,2,2048]{2,1,0:T(2,128)(2,1)S(1)}, u32[]{:S(2)}, u32[]{:S(2)}) async-start(bf16[16,2,2048]{2,1,0:T(2,128)(2,1)} %reshape.512), calls=%async_computation | async-start | bytes 262144 | tf_op jit(solution)/shard_map/all_to_all | solution.py:153
  98.9 6.2 %all-to-all-done = bf16[16,2,2048]{2,1,0:T(2,128)(2,1)S(1)} async-done(((bf16[16,2,2048]{2,1,0:T(2,128)(2,1)}), bf16[16,2,2048]{2,1,0:T(2,128)(2,1)S(1)}, u32[]{:S(2)}, u32[]{:S(2)}) %all-to-all-start) | async-done | bytes 131104 | tf_op jit(solution)/shard_map/all_to_all | solution.py:153
  110.6 156.8 %all_to_all.23 = bf16[16,9,2048]{2,1,0:T(8,128)(2,1)S(1)} all-to-all(bf16[16,9,2048]{2,1,0:T(8,128)(2,1)S(1)} %reshape.500), channel_id=1, replica_groups=mesh['sp'=16,'tp'=16] {'sp'}, dimensions={0} | all-to-all | bytes 1179648 | tf_op jit(solution)/shard_map/all_to_all | solution.py:176
  269.9 6.8 %collective-permute-done = bf16[144,2048]{1,0:T(8,128)(2,1)S(1)} collective-permute-done((bf16[144,2048]{1,0:T(8,128)(2,1)S(1)}, bf16[144,2048]{1,0:T(8,128)(2,1)S(1)}, u32[]{:S(2)}, u32[]{:S(2)}) %collective-permute-start) | collective-permute-done | bytes 589856 | tf_op jit(solution)/shard_map/ppermute | solution.py:188
  276.7 3.7 collective-permute-start.1
  280.4 6.8 %collective-permute-done.1 = bf16[144,2048]{1,0:T(8,128)(2,1)S(1)} collective-permute-done((bf16[144,2048]{1,0:T(8,128)(2,1)S(1)}, bf16[144,2048]{1,0:T(8,128)(2,1)S(1)}, u32[]{:S(2)}, u32[]{:S(2)}) %collective-permute-start.1) | collective-permute-done | bytes 589856 | tf_op jit(solution)/shard_map/ppermute | solution.py:188
  287.2 3.7 collective-permute-start.2
  290.9 6.8 %collective-permute-done.2 = bf16[144,2048]{1,0:T(8,128)(2,1)S(1)} collective-permute-done((bf16[144,2048]{1,0:T(8,128)(2,1)S(1)}, bf16[144,2048]{1,0:T(8,128)(2,1)S(1)}, u32[]{:S(2)}, u32[]{:S(2)}) %collective-permute-start.2) | collective-permute-done | bytes 589856 | tf_op jit(solution)/shard_map/ppermute | solution.py:188
  297.7 3.7 collective-permute-start.3
  302.3 6.0 %collective-permute-done.3 = bf16[144,2048]{1,0:T(8,128)(2,1)S(1)} collective-permute-done((bf16[144,2048]{1,0:T(8,128)(2,1)S(1)}, bf16[144,2048]{1,0:T(8,128)(2,1)S(1)}, u32[]{:S(2)}, u32[]{:S(2)}) %collective-permute-start.3) | collective-permute-done | bytes 589856 | tf_op jit(solution)/shard_map/ppermute | solution.py:188
  308.3 3.7 collective-permute-start.4
  313.6 5.1 %collective-permute-done.4 = bf16[144,2048]{1,0:T(8,128)(2,1)S(1)} collective-permute-done((bf16[144,2048]{1,0:T(8,128)(2,1)S(1)}, bf16[144,2048]{1,0:T(8,128)(2,1)S(1)}, u32[]{:S(2)}, u32[]{:S(2)}) %collective-permute-start.4) | collective-permute-done | bytes 589856 | tf_op jit(solution)/shard_map/ppermute | solution.py:188
  324.1 5.2 %collective-permute-done.5 = bf16[144,2048]{1,0:T(8,128)(2,1)S(1)} collective-permute-done((bf16[144,2048]{1,0:T(8,128)(2,1)S(1)}, bf16[144,2048]{1,0:T(8,128)(2,1)S(1)}, u32[]{:S(2)}, u32[]{:S(2)}) %collective-permute-start.5) | collective-permute-done | bytes 589856 | tf_op jit(solution)/shard_map/ppermute | solution.py:188
  334.8 5.1 %collective-permute-done.6 = bf16[144,2048]{1,0:T(8,128)(2,1)} collective-permute-done((bf16[144,2048]{1,0:T(8,128)(2,1)S(1)}, bf16[144,2048]{1,0:T(8,128)(2,1)}, u32[]{:S(2)}, u32[]{:S(2)}) %collective-permute-start.6) | collective-permute-done | bytes 589856 | tf_op jit(solution)/shard_map/ppermute | solution.py:188
  339.8 3.8 collective-permute-start.7
  345.6 5.2 %collective-permute-done.7 = bf16[144,2048]{1,0:T(8,128)(2,1)} collective-permute-done((bf16[144,2048]{1,0:T(8,128)(2,1)}, bf16[144,2048]{1,0:T(8,128)(2,1)}, u32[]{:S(2)}, u32[]{:S(2)}) %collective-permute-start.7) | collective-permute-done | bytes 589856 | tf_op jit(solution)/shard_map/ppermute | solution.py:188
  368.5 6.5 %copy-done.2 = bf16[4608,2048]{1,0:T(8,128)(2,1)} copy-done((bf16[4608,2048]{1,0:T(8,128)(2,1)}, bf16[4608,2048]{1,0:T(8,128)(2,1)S(1)}, u32[]{:S(2)}) %copy-start.2) | copy-done | bytes 18874392
  377.8 14.5 %convolution_convert_fusion = bf16[2304,2048]{1,0:T(8,128)(2,1)} fusion(f32[2304,128]{1,0:T(8,128)S(1)} %fusion.20, bf16[4608,2048]{1,0:T(8,128)(2,1)} %copy-done.2, s32[]{:T(128)S(6)} %select_n.49, bf16[1,128,2048]{2,1,0:T(8,128)(2,1)S(1)} %copy-done, bf16[1,2048,128]{2,1,0:T(8,128)(2,1)} %param.35), kind=kOutput, calls=%fused_computation.23 | convolution fusion | flops 2422407168 | bytes 21102596 | tf_op jit(solution)/shard_map/dot_general | solution.py:200
  392.3 71.3 %reduce-scatter.2.cloned.1.call-done = bf16[144,2048]{1,0:T(8,128)(2,1)} async-done(((bf16[2304,2048]{1,0:T(8,128)(2,1)}), bf16[144,2048]{1,0:T(8,128)(2,1)}) %reduce-scatter.2.cloned.1.call-update) | async-done | bytes 589840 | tf_op jit(solution)/shard_map/reduce_scatter | solution.py:199
  465.9 6.5 %all-to-all-start.2 = ((bf16[16,9,2048]{2,1,0:T(8,128)(2,1)}), bf16[16,9,2048]{2,1,0:T(8,128)(2,1)S(1)}, u32[]{:S(2)}, u32[]{:S(2)}) async-start(bf16[16,9,2048]{2,1,0:T(8,128)(2,1)} %reshape.502), calls=%async_computation.3 | async-start | bytes 2097152 | tf_op jit(solution)/shard_map/all_to_all | solution.py:205
  472.9 15.0 %all-to-all-done.2 = bf16[16,9,2048]{2,1,0:T(8,128)(2,1)S(1)} async-done(((bf16[16,9,2048]{2,1,0:T(8,128)(2,1)}), bf16[16,9,2048]{2,1,0:T(8,128)(2,1)S(1)}, u32[]{:S(2)}, u32[]{:S(2)}) %all-to-all-start.2) | async-done | bytes 589856 | tf_op jit(solution)/shard_map/all_to_all | solution.py:205
  (195 shorter events, 73.8 us)
Async XLA Ops:
  6.5 371.2 %copy-start = (bf16[1,128,2048]{2,1,0:T(8,128)(2,1)S(1)}, bf16[1,128,2048]{2,1,0:T(8,128)(2,1)}, u32[]{:S(2)}) copy-start(bf16[1,128,2048]{2,1,0:T(8,128)(2,1)} %param.37) | copy-start | bytes 1572868
  6.5 73.4 %all-gather.2.cloned.1.call-start = ((), (), s32[]{:S(2)}) async-start(), calls=%async_computation.4 | async-start | bytes 5570560 | tf_op jit(solution)/shard_map/all_gather | solution.py:114
  80.0 30.0 %copy-start.20 = (f32[2048]{0:T(1024)S(1)}, f32[2048]{0:T(1024)}, u32[]{:S(2)}) copy-start(f32[2048]{0:T(1024)} %param.32) | copy-start | bytes 24580
  91.0 14.1 %all-to-all-start = ((bf16[16,2,2048]{2,1,0:T(2,128)(2,1)}), bf16[16,2,2048]{2,1,0:T(2,128)(2,1)S(1)}, u32[]{:S(2)}, u32[]{:S(2)}) async-start(bf16[16,2,2048]{2,1,0:T(2,128)(2,1)} %reshape.512), calls=%async_computation | async-start | bytes 262144 | tf_op jit(solution)/shard_map/all_to_all | solution.py:153
  98.8 364.8 %reduce-scatter.2.cloned.1.call-start = ((), (), s32[]{:S(2)}) async-start(), calls=%async_computation.5 | async-start | bytes 10027008 | tf_op jit(solution)/shard_map/reduce_scatter | solution.py:199
  267.7 9.0 %collective-permute-start = (bf16[144,2048]{1,0:T(8,128)(2,1)S(1)}, bf16[144,2048]{1,0:T(8,128)(2,1)S(1)}, u32[]{:S(2)}, u32[]{:S(2)}) collective-permute-start(bf16[144,2048]{1,0:T(8,128)(2,1)S(1)} %reshape.501), channel_id=1, source_target_pairs={{0,1},{1,2},{2,3},{3,4},{4,5},{5,6},{6,7},{7,8},{8,9},{9,10},{10,1... | collective-permute-start | bytes 1769480 | tf_op jit(solution)/shard_map/ppermute | solution.py:188
  276.7 10.5 %collective-permute-start.1 = (bf16[144,2048]{1,0:T(8,128)(2,1)S(1)}, bf16[144,2048]{1,0:T(8,128)(2,1)S(1)}, u32[]{:S(2)}, u32[]{:S(2)}) collective-permute-start(bf16[144,2048]{1,0:T(8,128)(2,1)S(1)} %collective-permute-done), channel_id=1, source_target_pairs={{0,1},{1,2},{2,3},{3,4},{4,5},{5,6},{6,7},{7,8},{8,9},{9,10},{10,1... | collective-permute-start | bytes 1769480 | tf_op jit(solution)/shard_map/ppermute | solution.py:188
  280.4 10.5 %collective-permute-start.8 = (bf16[144,2048]{1,0:T(8,128)(2,1)S(1)}, bf16[144,2048]{1,0:T(8,128)(2,1)S(1)}, u32[]{:S(2)}, u32[]{:S(2)}) collective-permute-start(bf16[144,2048]{1,0:T(8,128)(2,1)S(1)} %reshape.501), channel_id=1, source_target_pairs={{0,15},{1,0},{2,1},{3,2},{4,3},{5,4},{6,5},{7,6},{8,7},{9,8},{10,9... | collective-permute-start | bytes 1769480 | tf_op jit(solution)/shard_map/ppermute | solution.py:191
  287.2 10.5 %collective-permute-start.2 = (bf16[144,2048]{1,0:T(8,128)(2,1)S(1)}, bf16[144,2048]{1,0:T(8,128)(2,1)S(1)}, u32[]{:S(2)}, u32[]{:S(2)}) collective-permute-start(bf16[144,2048]{1,0:T(8,128)(2,1)S(1)} %collective-permute-done.1), channel_id=1, source_target_pairs={{0,1},{1,2},{2,3},{3,4},{4,5},{5,6},{6,7},{7,8},{8,9},{9,10},{10,1... | collective-permute-start | bytes 1769480 | tf_op jit(solution)/shard_map/ppermute | solution.py:188
  290.9 10.5 %collective-permute-start.9 = (bf16[144,2048]{1,0:T(8,128)(2,1)S(1)}, bf16[144,2048]{1,0:T(8,128)(2,1)S(1)}, u32[]{:S(2)}, u32[]{:S(2)}) collective-permute-start(bf16[144,2048]{1,0:T(8,128)(2,1)S(1)} %collective-permute-done.8), channel_id=1, source_target_pairs={{0,15},{1,0},{2,1},{3,2},{4,3},{5,4},{6,5},{7,6},{8,7},{9,8},{10,9... | collective-permute-start | bytes 1769480 | tf_op jit(solution)/shard_map/ppermute | solution.py:191
  297.7 10.5 %collective-permute-start.3 = (bf16[144,2048]{1,0:T(8,128)(2,1)S(1)}, bf16[144,2048]{1,0:T(8,128)(2,1)S(1)}, u32[]{:S(2)}, u32[]{:S(2)}) collective-permute-start(bf16[144,2048]{1,0:T(8,128)(2,1)S(1)} %collective-permute-done.2), channel_id=1, source_target_pairs={{0,1},{1,2},{2,3},{3,4},{4,5},{5,6},{6,7},{7,8},{8,9},{9,10},{10,1... | collective-permute-start | bytes 1769480 | tf_op jit(solution)/shard_map/ppermute | solution.py:188
  302.3 10.5 %collective-permute-start.10 = (bf16[144,2048]{1,0:T(8,128)(2,1)S(1)}, bf16[144,2048]{1,0:T(8,128)(2,1)S(1)}, u32[]{:S(2)}, u32[]{:S(2)}) collective-permute-start(bf16[144,2048]{1,0:T(8,128)(2,1)S(1)} %collective-permute-done.9), channel_id=1, source_target_pairs={{0,15},{1,0},{2,1},{3,2},{4,3},{5,4},{6,5},{7,6},{8,7},{9,8},{10,9... | collective-permute-start | bytes 1769480 | tf_op jit(solution)/shard_map/ppermute | solution.py:191
  308.3 10.5 %collective-permute-start.4 = (bf16[144,2048]{1,0:T(8,128)(2,1)S(1)}, bf16[144,2048]{1,0:T(8,128)(2,1)S(1)}, u32[]{:S(2)}, u32[]{:S(2)}) collective-permute-start(bf16[144,2048]{1,0:T(8,128)(2,1)S(1)} %collective-permute-done.3), channel_id=1, source_target_pairs={{0,1},{1,2},{2,3},{3,4},{4,5},{5,6},{6,7},{7,8},{8,9},{9,10},{10,1... | collective-permute-start | bytes 1769480 | tf_op jit(solution)/shard_map/ppermute | solution.py:188
  312.8 10.5 %collective-permute-start.11 = (bf16[144,2048]{1,0:T(8,128)(2,1)S(1)}, bf16[144,2048]{1,0:T(8,128)(2,1)S(1)}, u32[]{:S(2)}, u32[]{:S(2)}) collective-permute-start(bf16[144,2048]{1,0:T(8,128)(2,1)S(1)} %collective-permute-done.10), channel_id=1, source_target_pairs={{0,15},{1,0},{2,1},{3,2},{4,3},{5,4},{6,5},{7,6},{8,7},{9,8},{10,9... | collective-permute-start | bytes 1769480 | tf_op jit(solution)/shard_map/ppermute | solution.py:191
  318.8 10.5 %collective-permute-start.5 = (bf16[144,2048]{1,0:T(8,128)(2,1)S(1)}, bf16[144,2048]{1,0:T(8,128)(2,1)S(1)}, u32[]{:S(2)}, u32[]{:S(2)}) collective-permute-start(bf16[144,2048]{1,0:T(8,128)(2,1)S(1)} %collective-permute-done.4), channel_id=1, source_target_pairs={{0,1},{1,2},{2,3},{3,4},{4,5},{5,6},{6,7},{7,8},{8,9},{9,10},{10,1... | collective-permute-start | bytes 1769480 | tf_op jit(solution)/shard_map/ppermute | solution.py:188
  324.1 10.6 %collective-permute-start.12 = (bf16[144,2048]{1,0:T(8,128)(2,1)S(1)}, bf16[144,2048]{1,0:T(8,128)(2,1)}, u32[]{:S(2)}, u32[]{:S(2)}) collective-permute-start(bf16[144,2048]{1,0:T(8,128)(2,1)S(1)} %collective-permute-done.11), channel_id=1, source_target_pairs={{0,15},{1,0},{2,1},{3,2},{4,3},{5,4},{6,5},{7,6},{8,7},{9,8},{10,9... | collective-permute-start | bytes 1769480 | tf_op jit(solution)/shard_map/ppermute | solution.py:191
  329.3 10.5 %collective-permute-start.6 = (bf16[144,2048]{1,0:T(8,128)(2,1)S(1)}, bf16[144,2048]{1,0:T(8,128)(2,1)}, u32[]{:S(2)}, u32[]{:S(2)}) collective-permute-start(bf16[144,2048]{1,0:T(8,128)(2,1)S(1)} %collective-permute-done.5), channel_id=1, source_target_pairs={{0,1},{1,2},{2,3},{3,4},{4,5},{5,6},{6,7},{7,8},{8,9},{9,10},{10,1... | collective-permute-start | bytes 1769480 | tf_op jit(solution)/shard_map/ppermute | solution.py:188
  334.8 10.8 %collective-permute-start.13 = (bf16[144,2048]{1,0:T(8,128)(2,1)}, bf16[144,2048]{1,0:T(8,128)(2,1)}, u32[]{:S(2)}, u32[]{:S(2)}) collective-permute-start(bf16[144,2048]{1,0:T(8,128)(2,1)} %collective-permute-done.12), channel_id=1, source_target_pairs={{0,15},{1,0},{2,1},{3,2},{4,3},{5,4},{6,5},{7,6},{8,7},{9,8},{10,9... | collective-permute-start | bytes 1769480 | tf_op jit(solution)/shard_map/ppermute | solution.py:191
  339.8 10.9 %collective-permute-start.7 = (bf16[144,2048]{1,0:T(8,128)(2,1)}, bf16[144,2048]{1,0:T(8,128)(2,1)}, u32[]{:S(2)}, u32[]{:S(2)}) collective-permute-start(bf16[144,2048]{1,0:T(8,128)(2,1)} %collective-permute-done.6), channel_id=1, source_target_pairs={{0,1},{1,2},{2,3},{3,4},{4,5},{5,6},{6,7},{7,8},{8,9},{9,10},{10,1... | collective-permute-start | bytes 1769480 | tf_op jit(solution)/shard_map/ppermute | solution.py:188
  343.7 31.3 %copy-start.22 = (bf16[1,2048,128]{2,1,0:T(8,128)(2,1)S(1)}, bf16[1,2048,128]{2,1,0:T(8,128)(2,1)}, u32[]{:S(2)}) copy-start(bf16[1,2048,128]{2,1,0:T(8,128)(2,1)} %param.36) | copy-start | bytes 1572868
  345.6 17.7 %collective-permute-start.14 = (bf16[144,2048]{1,0:T(8,128)(2,1)}, bf16[144,2048]{1,0:T(8,128)(2,1)S(1)}, u32[]{:S(2)}, u32[]{:S(2)}) collective-permute-start(bf16[144,2048]{1,0:T(8,128)(2,1)} %collective-permute-done.13), channel_id=1, source_target_pairs={{0,15},{1,0},{2,1},{3,2},{4,3},{5,4},{6,5},{7,6},{8,7},{9,8},{10,9... | collective-permute-start | bytes 1769480 | tf_op jit(solution)/shard_map/ppermute | solution.py:191
  377.7 95.0 %copy-start.21 = (f32[64,2]{0,1:T(2,128)S(1)}, f32[64,2]{0,1:T(2,128)}, u32[]{:S(2)}) copy-start(f32[64,2]{0,1:T(2,128)} %param.34) | copy-start | bytes 1540
  377.7 114.0 %copy-start.18 = (bf16[64,2048]{1,0:T(8,128)(2,1)S(1)}, bf16[64,2048]{1,0:T(8,128)(2,1)}, u32[]{:S(2)}) copy-start(bf16[64,2048]{1,0:T(8,128)(2,1)} %param.31) | copy-start | bytes 786436
  465.9 22.0 %all-to-all-start.2 = ((bf16[16,9,2048]{2,1,0:T(8,128)(2,1)}), bf16[16,9,2048]{2,1,0:T(8,128)(2,1)S(1)}, u32[]{:S(2)}, u32[]{:S(2)}) async-start(bf16[16,9,2048]{2,1,0:T(8,128)(2,1)} %reshape.502), calls=%async_computation.3 | async-start | bytes 2097152 | tf_op jit(solution)/shard_map/all_to_all | solution.py:205
  (18 other events, 283.0 us)
Sparse Core Ops, SparseCore 0:
  16.9 62.9 all-gather.1
  392.4 71.1 reduce-scatter.1
